TPU v7x, 32 devices: a whole 2x2x4 slice. The times are simulated.
32 devices in a mesh: rep: 2 (over x), fs: 4 (over y, core), tp: 4 (over z).
Axes of the slice: x: 2, y: 2, z: 4, core: 2. Of those that a mesh axis runs over, the one named last changes fastest.
Arguments:
- inputs: bfloat16 [4096, 4096], P(('rep', 'fs', 'tp')), may hold values from -6 to 6
- w_gate: bfloat16 [4096, 11008], P('fs', 'tp'), may hold values from -0.09375 to 0.09375
- w_up: bfloat16 [4096, 11008], P('fs', 'tp'), may hold values from -0.09375 to 0.09375
- w_down: bfloat16 [11008, 4096], P('tp', 'fs'), may hold values from -0.0546875 to 0.0546875
- d_out: bfloat16 [4096, 4096], P(('rep', 'fs', 'tp')), may hold values from -6 to 6
Outputs:
- grad_inputs: bfloat16 [4096, 4096], P(('rep', 'fs', 'tp'))
- grad_gate: float32 [4096, 11008], P('fs', 'tp')
- grad_up: float32 [4096, 11008], P('fs', 'tp')
- grad_down: float32 [11008, 4096], P('tp', 'fs')
All inputs are finite; a program needn't handle non-finite values.
Results may differ from a plain program's by a relative error of at most 0.00185.
Values may be sent and summed in bfloat16 or wider, within the bound.
A program may use at most 448 MiB of HBM per device.

v0:
```python
import jax
import jax.numpy as jnp
from jax import lax
from jax.sharding import PartitionSpec as P


def scattered(term, extent, axis):
    whole = term(jnp.int32(0), extent * lax.axis_size(axis))
    return lax.psum_scatter(whole, axis, scatter_dimension=0, tiled=True)


def stored(values):
    return lax.optimization_barrier(values.astype(jnp.bfloat16)).astype(jnp.float32)


def times_t(left, right):
    return lax.dot_general(
        left, right, (((1,), (1,)), ((), ())), preferred_element_type=jnp.float32
    )


def across_rows(left, right):
    return lax.dot_general(
        left, right, (((0,), (0,)), ((), ())), preferred_element_type=jnp.float32
    )


def local(inputs, w_gate, w_up, w_down, d_out):
    rows_in, rows_out = (
        lax.all_gather(inputs, "tp", axis=0, tiled=True),
        lax.all_gather(d_out, "tp", axis=0, tiled=True),
    )
    down_t = w_down.T
    columns = w_gate.shape[1]
    full_gate, full_up, full_down = (
        lax.all_gather(w_gate, "fs", axis=0, tiled=True),
        lax.all_gather(w_up, "fs", axis=0, tiled=True),
        lax.all_gather(down_t, "fs", axis=0, tiled=True),
    )
    gate_acc = jnp.dot(rows_in, full_gate, preferred_element_type=jnp.float32)
    up_acc = jnp.dot(rows_in, full_up, preferred_element_type=jnp.float32)
    back_acc = jnp.dot(rows_out, full_down, preferred_element_type=jnp.float32)
    gate_val = stored(gate_acc)
    up_val = stored(up_acc)
    back_val = stored(back_acc)
    sigma = jax.nn.sigmoid(gate_val)
    active = gate_val * sigma
    hidden = (active * up_val).astype(jnp.bfloat16)
    d_gate = (back_val * up_val * sigma * (1.0 + gate_val * (1.0 - sigma))).astype(jnp.bfloat16)
    d_up = (back_val * active).astype(jnp.bfloat16)
    share = rows_in.shape[0] // lax.axis_size("tp")

    def input_rows(start, count):
        part_gate = lax.dynamic_slice_in_dim(d_gate, start, count, 0)
        part_up = lax.dynamic_slice_in_dim(d_up, start, count, 0)
        return times_t(part_gate, full_gate) + times_t(part_up, full_up)

    grad_inputs = scattered(input_rows, share, "tp")
    grad_inputs = grad_inputs.astype(jnp.bfloat16)

    def weight_rows(start, count):
        part_in = lax.dynamic_slice_in_dim(rows_in, start, count, 1)
        part_out = lax.dynamic_slice_in_dim(rows_out, start, count, 1)
        return jnp.concatenate(
            [
                across_rows(part_in, d_gate),
                across_rows(part_in, d_up),
                across_rows(part_out, hidden),
            ],
            axis=1,
        )

    block = rows_in.shape[1] // (lax.axis_size("fs") * lax.axis_size("rep"))
    summed = scattered(weight_rows, block, ("fs", "rep"))
    summed = lax.all_gather(summed, "rep", axis=0, tiled=True)
    grad_gate = summed[:, :columns]
    grad_up = summed[:, columns : 2 * columns]
    grad_down = summed[:, 2 * columns :].T
    return (grad_inputs, grad_gate, grad_up, grad_down)


def solution(mesh):
    return jax.shard_map(
        local,
        mesh=mesh,
        in_specs=(
            P(("rep", "fs", "tp"), None),
            P("fs", "tp"),
            P("fs", "tp"),
            P("tp", "fs"),
            P(("rep", "fs", "tp"), None),
        ),
        out_specs=(P(("rep", "fs", "tp"), None), P("fs", "tp"), P("fs", "tp"), P("tp", "fs")),
        check_vma=False,
    )
```

profile of v0, /device:TPU:0, one launch (start us, length us, event | category | flops | bytes accessed | tf_op | source)
XLA Modules:
  0.0 2122.0 jit_solution(17381988144722497567)
XLA Ops:
  7.2 0.0 all-gather.7.cloned.1.call-start
  7.2 0.7 all-gather.7.cloned.1.call-update
  7.9 0.0 all-gather.9.cloned.1.call-start
  7.9 0.7 all-gather.9.cloned.1.call-update
  8.6 0.0 all-gather.11.cloned.1.call-start
  8.7 0.7 all-gather.11.cloned.1.call-update
  9.4 0.0 all-gather.13.cloned.1.call-start
  9.4 0.5 all-gather.13.cloned.1.call-update
  10.0 0.0 all-gather.15.cloned.1.call-start
  10.0 0.5 all-gather.15.cloned.1.call-update
  10.5 0.0 reduce-scatter.5.cloned.1.call-start
  10.6 81.9 %all-gather.7.cloned.1.call-done = bf16[512,4096]{1,0:T(8,128)(2,1)} async-done(((bf16[128,4096]{1,0:T(8,128)(2,1)}), bf16[512,4096]{1,0:T(8,128)(2,1)}) %all-gather.7.cloned.1.call-update) | async-done | bytes 4194320 | tf_op jit(solution)/shard_map/all_gather | solution.py:31
  92.5 140.6 %all-gather.9.cloned.1.call-done = bf16[4096,2752]{0,1:T(8,128)(2,1)} async-done(((bf16[1024,2752]{0,1:T(8,128)(2,1)}), bf16[4096,2752]{0,1:T(8,128)(2,1)}) %all-gather.9.cloned.1.call-update) | async-done | bytes 22544400 | tf_op jit(solution)/shard_map/all_gather | solution.py:38
  233.1 17.5 convolution_convert_fusion.2
  250.6 64.2 %all-gather.11.cloned.1.call-done = bf16[512,4096]{1,0:T(8,128)(2,1)} async-done(((bf16[128,4096]{1,0:T(8,128)(2,1)}), bf16[512,4096]{1,0:T(8,128)(2,1)}) %all-gather.11.cloned.1.call-update) | async-done | bytes 4194320 | tf_op jit(solution)/shard_map/all_gather | solution.py:30
  314.8 140.5 %all-gather.13.cloned.1.call-done = bf16[4096,2752]{0,1:T(8,128)(2,1)} async-done(((bf16[1024,2752]{0,1:T(8,128)(2,1)}), bf16[4096,2752]{0,1:T(8,128)(2,1)}) %all-gather.13.cloned.1.call-update) | async-done | bytes 22544400 | tf_op jit(solution)/shard_map/all_gather | solution.py:37
  455.3 18.6 convolution_convert_fusion.1
  473.9 123.1 %all-gather.15.cloned.1.call-done = bf16[4096,2752]{0,1:T(8,128)(2,1)} async-done(((bf16[1024,2752]{0,1:T(8,128)(2,1)}), bf16[4096,2752]{0,1:T(8,128)(2,1)}) %all-gather.15.cloned.1.call-update) | async-done | bytes 22544400 | tf_op jit(solution)/shard_map/all_gather | solution.py:36
  596.9 19.1 convolution_convert_fusion
  616.0 23.5 %convolution_bitcast_fusion = f32[4096,2752]{0,1:T(8,128)} fusion(bf16[512,4096]{1,0:T(8,128)(2,1)} %all-gather.7.cloned.1.call-done, bf16[512,2752]{0,1:T(8,128)(2,1)} %convolution_convert_fusion.1, bf16[512,2752]{0,1:T(8,128)(2,1)} %convolution_convert_fusion), kind=kOutput, calls=%fused_computation.1 | convolution fusion | flops 11553996800 | bytes 54919168 | tf_op jit(solution)/shard_map/dot_general | solution.py:23
  639.6 24.1 %convolution_bitcast_fusion.2 = f32[4096,2752]{0,1:T(8,128)} fusion(bf16[512,4096]{1,0:T(8,128)(2,1)} %all-gather.11.cloned.1.call-done, bf16[512,2752]{0,1:T(8,128)(2,1)} %convolution_convert_fusion.1, bf16[512,2752]{0,1:T(8,128)(2,1)S(1)} %convolution_convert_fusion.2, bf16[512,2752]{0,1:T(8,128)(2,1)} %convolution_convert_fusion), kind=kOutput, calls=%fused_computation.3 | convolution fusion | flops 11561041920 | bytes 57737216 | tf_op jit(solution)/shard_map/dot_general | solution.py:23
  663.7 23.1 %convolution_bitcast_fusion.1 = f32[4096,2752]{0,1:T(8,128)} fusion(bf16[512,4096]{1,0:T(8,128)(2,1)} %all-gather.11.cloned.1.call-done, bf16[512,2752]{0,1:T(8,128)(2,1)S(1)} %convolution_convert_fusion.2, bf16[512,2752]{0,1:T(8,128)(2,1)} %convolution_convert_fusion), kind=kOutput, calls=%fused_computation.2 | convolution fusion | flops 11553996800 | bytes 54919168 | tf_op jit(solution)/shard_map/dot_general | solution.py:23
  686.8 110.7 %pad_maximum_fusion = f32[4096,8256]{0,1:T(8,128)} fusion(f32[4096,2752]{0,1:T(8,128)} %convolution_bitcast_fusion, f32[4096,2752]{0,1:T(8,128)} %convolution_bitcast_fusion.1, f32[4096,2752]{0,1:T(8,128)} %convolution_bitcast_fusion.2), kind=kLoop, calls=%fused_computation | loop fusion | flops 67633152 | bytes 270532608 | tf_op jit(solution)/shard_map/concatenate | solution.py:64
  797.5 0.0 reduce-scatter.5.cloned.1.call-update
  797.5 0.0 reduce-scatter.3.cloned.1.call-start
  797.5 0.0 copy-start
  797.6 26.8 %fusion.14 = f32[512,4096]{1,0:T(8,128)} fusion(bf16[4096,2752]{0,1:T(8,128)(2,1)} %all-gather.15.cloned.1.call-done, bf16[512,2752]{0,1:T(8,128)(2,1)} %convolution_convert_fusion.1, bf16[512,2752]{0,1:T(8,128)(2,1)S(1)} %convolution_convert_fusion.2, bf16[512,2752]{0,1:T(8,128)(2,1)} %convolution_convert_fusion), kind=kOutput, calls=%fused_computation.25 | convolution fusion | flops 11561041920 | bytes 39387136 | tf_op jit(solution)/shard_map/dot_general | solution.py:17
  824.3 0.0 copy-done
  824.3 20.7 convolution_add_fusion
  845.0 0.0 reduce-scatter.3.cloned.1.call-update
  845.0 0.0 all-gather.17.cloned.1.call-start
  845.1 701.2 %reduce-scatter.5.cloned.1.call-done = f32[512,8256]{0,1:T(8,128)} async-done(((f32[4096,8256]{0,1:T(8,128)}), f32[512,8256]{0,1:T(8,128)}) %reduce-scatter.5.cloned.1.call-update) | async-done | bytes 16908304 | tf_op jit(solution)/shard_map/reduce_scatter | solution.py:9
  1546.2 0.0 all-gather.17.cloned.1.call-update
  1546.3 147.1 %reduce-scatter.3.cloned.1.call-done = f32[128,4096]{1,0:T(8,128)} async-done(((f32[512,4096]{1,0:T(8,128)}), f32[128,4096]{1,0:T(8,128)}) %reduce-scatter.3.cloned.1.call-update) | async-done | bytes 2097168 | tf_op jit(solution)/shard_map/reduce_scatter | solution.py:9
  1693.4 2.7 convert_element_type.38
  1696.1 393.2 %all-gather.17.cloned.1.call-done = f32[1024,8256]{0,1:T(8,128)} async-done(((f32[512,8256]{0,1:T(8,128)}), f32[1024,8256]{0,1:T(8,128)}) %all-gather.17.cloned.1.call-update) | async-done | bytes 33816592 | tf_op jit(solution)/shard_map/all_gather | solution.py:75
  2089.3 25.5 %slice_bitcast_fusion = (f32[2752,1024]{1,0:T(8,128)}, f32[1024,2752]{0,1:T(8,128)}, f32[1024,2752]{0,1:T(8,128)}) fusion(f32[1024,8256]{0,1:T(8,128)} %all-gather.17.cloned.1.call-done), kind=kLoop, calls=%fused_computation.4 | loop fusion | bytes 67633152 | tf_op jit(solution)/shard_map/transpose | solution.py:78
Async XLA Ops:
  7.2 85.3 %all-gather.7.cloned.1.call-start = ((), (), s32[]{:S(2)}) async-start(), calls=%async_computation.2 | async-start | bytes 5242880 | tf_op jit(solution)/shard_map/all_gather | solution.py:31
  7.9 225.2 %all-gather.9.cloned.1.call-start = ((), (), s32[]{:S(2)}) async-start(), calls=%async_computation.3 | async-start | bytes 28180480 | tf_op jit(solution)/shard_map/all_gather | solution.py:38
  8.6 306.2 %all-gather.11.cloned.1.call-start = ((), (), s32[]{:S(2)}) async-start(), calls=%async_computation.4 | async-start | bytes 5242880 | tf_op jit(solution)/shard_map/all_gather | solution.py:30
  9.4 445.9 %all-gather.13.cloned.1.call-start = ((), (), s32[]{:S(2)}) async-start(), calls=%async_computation.5 | async-start | bytes 28180480 | tf_op jit(solution)/shard_map/all_gather | solution.py:37
  10.0 587.0 %all-gather.15.cloned.1.call-start = ((), (), s32[]{:S(2)}) async-start(), calls=%async_computation.6 | async-start | bytes 28180480 | tf_op jit(solution)/shard_map/all_gather | solution.py:36
  10.5 1535.7 %reduce-scatter.5.cloned.1.call-start = ((), (), s32[]{:S(2)}) async-start(), calls=%async_computation.8 | async-start | bytes 152174592 | tf_op jit(solution)/shard_map/reduce_scatter | solution.py:9
  797.5 895.9 %reduce-scatter.3.cloned.1.call-start = ((), (), s32[]{:S(2)}) async-start(), calls=%async_computation.7 | async-start | bytes 10485760 | tf_op jit(solution)/shard_map/reduce_scatter | solution.py:9
  797.5 26.8 %copy-start = (bf16[512,2752]{0,1:T(8,128)(2,1)S(1)}, bf16[512,2752]{0,1:T(8,128)(2,1)}, u32[]{:S(2)}) copy-start(bf16[512,2752]{0,1:T(8,128)(2,1)} %convolution_convert_fusion) | copy-start | bytes 8454148
  845.0 1244.2 %all-gather.17.cloned.1.call-start = ((), (), s32[]{:S(2)}) async-start(), calls=%async_computation.9 | async-start | bytes 50724864 | tf_op jit(solution)/shard_map/all_gather | solution.py:75
Sparse Core Ops, SparseCore 0:
  9.5 82.8 all-gather.6
  94.0 138.9 all-gather.8
  234.6 80.1 all-gather.10
  316.2 138.9 all-gather.12
  456.7 140.1 all-gather.14
  797.6 748.5 reduce-scatter.4
  1549.2 144.1 reduce-scatter.2
  1694.9 394.2 all-gather.16
where the time goes:
time: 2130 us; the launch traced here: 2120 us
  waiting for transfers between devices  1790 us (84%)
  matrix products  173 us (8%)
  other arithmetic  113 us (5%)
  local copies, waits for them, and re-layouts  25.5 us (1%)
    reduce_scatter x2, waiting for transfers between devices, scattered(): return lax.psum_scatter(whole, axis, scatter_dimension=0, tiled=True)  848 us
    all_gather x1, waiting for transfers between devices, local(): summed = lax.all_gather(summed, 'rep', axis=0, tiled=True)  393 us
    all_gather x1, waiting for transfers between devices, local(): lax.all_gather(down_t, 'fs', axis=0, tiled=True)  141 us
    all_gather x1, waiting for transfers between devices, local(): lax.all_gather(w_up, 'fs', axis=0, tiled=True)  140 us
    all_gather x1, waiting for transfers between devices, local(): lax.all_gather(w_gate, 'fs', axis=0, tiled=True)  123 us
    concatenate x1, other arithmetic, weight_rows(): jnp.concatenate([across_rows(part_in, d_gate), across_rows(part_in, d_up)...  111 us
    all_gather x1, waiting for transfers between devices, local(): lax.all_gather(d_out, 'tp', axis=0, tiled=True)  81.9 us
    dot_general x3, matrix products, across_rows(): lax.dot_general(left, right, (((0,), (0,)), ((), ())), preferred_element_...  70.8 us
  transfers between devices with their start and end apart: 8, of which 8 were waited for; matrix products, arithmetic and copies ran while one was open for 4% of the time, Pallas kernels for 0%

commit v1 on v0

v1 whole, which is shorter than its diff:
```python
import jax
import jax.numpy as jnp
from jax import lax
from jax.sharding import PartitionSpec as P


def stored(values):
    return lax.optimization_barrier(values.astype(jnp.bfloat16)).astype(jnp.float32)


def times_t(left, right):
    return lax.dot_general(
        left, right, (((1,), (1,)), ((), ())), preferred_element_type=jnp.float32
    )


def across_rows(left, right):
    return lax.dot_general(
        left, right, (((0,), (0,)), ((), ())), preferred_element_type=jnp.float32
    )


def whole_rows(shard):
    half = shard.shape[0] // lax.axis_size("rep")
    part = lax.dynamic_slice_in_dim(shard, lax.axis_index("rep") * half, half, 0)
    return lax.all_gather(part, ("fs", "rep"), axis=0, tiled=True)


def all_tokens(rows):
    return lax.all_gather(rows, ("rep", "fs"), axis=0, tiled=True)


def own_columns(shard):
    tokens = shard.shape[0]
    fs, tp, rep = lax.axis_size("fs"), lax.axis_size("tp"), lax.axis_size("rep")
    part = lax.all_to_all(shard, "fs", split_axis=1, concat_axis=0, tiled=True)
    part = lax.all_gather(part, ("rep", "tp"), axis=0, tiled=True)
    width = part.shape[1]
    part = part.reshape(rep, tp, fs, tokens, width).transpose(0, 2, 1, 3, 4)
    return part.reshape(rep * fs * tp * tokens, width)


def local(inputs, w_gate, w_up, w_down, d_out):
    rows_in = lax.all_gather(inputs, "tp", axis=0, tiled=True)
    full_gate = whole_rows(w_gate)
    full_up = whole_rows(w_up)
    rows_out = lax.all_gather(d_out, "tp", axis=0, tiled=True)
    full_down = whole_rows(w_down.T)
    gate_val = stored(jnp.dot(rows_in, full_gate, preferred_element_type=jnp.float32))
    up_val = stored(jnp.dot(rows_in, full_up, preferred_element_type=jnp.float32))
    sigma = jax.nn.sigmoid(gate_val)
    active = gate_val * sigma
    hidden = (active * up_val).astype(jnp.bfloat16)
    back_val = stored(jnp.dot(rows_out, full_down, preferred_element_type=jnp.float32))
    d_gate = (back_val * up_val * sigma * (1.0 + gate_val * (1.0 - sigma))).astype(jnp.bfloat16)
    d_up = (back_val * active).astype(jnp.bfloat16)

    cols_in = own_columns(inputs)
    cols_out = own_columns(d_out)
    grad_down = across_rows(all_tokens(hidden), cols_out)
    grad_gate = across_rows(cols_in, all_tokens(d_gate))
    grad_up = across_rows(cols_in, all_tokens(d_up))

    grad_inputs = times_t(d_gate, full_gate) + times_t(d_up, full_up)
    grad_inputs = lax.psum_scatter(grad_inputs, "tp", scatter_dimension=0, tiled=True)
    grad_inputs = grad_inputs.astype(jnp.bfloat16)
    return (grad_inputs, grad_gate, grad_up, grad_down)


def solution(mesh):
    return jax.shard_map(
        local,
        mesh=mesh,
        in_specs=(
            P(("rep", "fs", "tp"), None),
            P("fs", "tp"),
            P("fs", "tp"),
            P("tp", "fs"),
            P(("rep", "fs", "tp"), None),
        ),
        out_specs=(P(("rep", "fs", "tp"), None), P("fs", "tp"), P("fs", "tp"), P("tp", "fs")),
        check_vma=False,
    )
```

time: 2130 us -> 1330 us (0.62)
  waiting for transfers between devices: 1790 us -> 1050 us
  other arithmetic: 113 us -> 9.11 us
  blocking collectives: 0 us -> 35.4 us
    reduce_scatter x2 -> x1, waiting for transfers between devices: 848 us -> 137 us  [local(): lax.psum_scatter(grad_inputs, 'tp', scatter_dimension=0, tiled=True)]
    concatenate x1 -> x0, other arithmetic: 111 us -> none  [weight_rows(): jnp.concatenate([across_rows(part_in, d_gate), across_rows(part_in, d_up)...]
    all_to_all x0 -> x2, blocking collectives: none -> 35.4 us  [own_columns(): part = lax.all_to_all(shard, 'fs', split_axis=1, concat_axis=0, tiled=True)]
    all_gather x6 -> x10, waiting for transfers between devices: 943 us -> 912 us  [the longest x3 341 us: whole_rows(): return lax.all_gather(part, ('fs', 'rep'), axis=0, tiled=True)]
    transpose x1 -> x0, local copies, waits for them, and re-layouts: 25.5 us -> none  [local(): grad_down = summed[:, 2 * columns:].T]
  transfers between devices with their start and end apart: 8 -> 11, of which waited for: 8 -> 11; matrix products, arithmetic and copies ran while one was open for 4% -> 15% of each run, Pallas kernels for 0% -> 0%
where the time goes in v1:
time: 1330 us
  waiting for transfers between devices  1050 us (79%)
  matrix products  188 us (14%)
  blocking collectives  35.4 us (3%)
  local copies, waits for them, and re-layouts  31.2 us (2%)
  between operations  14.2 us (1%)
    all_gather x3, waiting for transfers between devices, whole_rows(): return lax.all_gather(part, ('fs', 'rep'), axis=0, tiled=True)  341 us
    all_gather x3, waiting for transfers between devices, all_tokens(): return lax.all_gather(rows, ('rep', 'fs'), axis=0, tiled=True)  299 us
    all_gather x2, waiting for transfers between devices, own_columns(): part = lax.all_gather(part, ('rep', 'tp'), axis=0, tiled=True)  176 us
    reduce_scatter x1, waiting for transfers between devices, local(): lax.psum_scatter(grad_inputs, 'tp', scatter_dimension=0, tiled=True)  137 us
    dot_general x3, matrix products, across_rows(): lax.dot_general(left, right, (((0,), (0,)), ((), ())), preferred_element_...  91.8 us
    all_gather x1, waiting for transfers between devices, local(): rows_out = lax.all_gather(d_out, 'tp', axis=0, tiled=True)  63 us
    dot_general x2, matrix products, times_t(): lax.dot_general(left, right, (((1,), (1,)), ((), ())), preferred_element_...  40.4 us
    all_to_all x2, blocking collectives, own_columns(): part = lax.all_to_all(shard, 'fs', split_axis=1, concat_axis=0, tiled=True)  35.4 us
  transfers between devices with their start and end apart: 11, of which 11 were waited for; matrix products, arithmetic and copies ran while one was open for 15% of the time, Pallas kernels for 0%

profile of v1, /device:TPU:0, one launch (start us, length us, event | category | flops | bytes accessed | tf_op | source)
XLA Modules:
  0.0 1330.6 jit_solution(2855823850604729302)
XLA Ops:
  7.2 0.0 all-gather.17.cloned.1.call-start
  7.2 0.7 all-gather.17.cloned.1.call-update
  7.9 0.0 all-gather.15.cloned.1.call-start
  8.0 3.5 constant_dynamic-slice_fusion.1
  11.5 0.0 all-gather.19.cloned.1.call-start
  11.6 3.5 constant_dynamic-slice_fusion
  15.1 0.0 all-gather.13.cloned.1.call-start
  15.2 0.5 all-gather.13.cloned.1.call-update
  15.7 0.0 all-gather.11.cloned.1.call-start
  15.8 3.5 dynamic-slice_bitcast_fusion
  19.3 0.0 all-gather.23.cloned.1.call-start
  19.4 0.7 copy.11
  20.1 18.5 %all_to_all.38 = bf16[128,4,1024]{0,2,1:T(8,128)(2,1)S(1)} all-to-all(bf16[128,4,1024]{0,2,1:T(8,128)(2,1)S(1)} %bitcast.51), channel_id=1, replica_groups=mesh['rep'=2,'fs'=4,'tp'=4] {'fs'}, dimensions={1} | all-to-all | bytes 2097152 | tf_op jit(solution)/shard_map/all_to_all | solution.py:36
  38.6 1.3 copy.12
  39.9 0.0 all-gather.29.cloned.1.call-start
  40.0 0.7 copy.14
  40.6 16.9 %all_to_all.39 = bf16[128,4,1024]{0,2,1:T(8,128)(2,1)S(1)} all-to-all(bf16[128,4,1024]{0,2,1:T(8,128)(2,1)S(1)} %bitcast.52), channel_id=1, replica_groups=mesh['rep'=2,'fs'=4,'tp'=4] {'fs'}, dimensions={1} | all-to-all | bytes 2097152 | tf_op jit(solution)/shard_map/all_to_all | solution.py:36
  57.5 1.3 copy.15
  58.8 0.4 reduce-scatter.2.cloned.1.call-start
  59.2 33.3 %all-gather.17.cloned.1.call-done = bf16[512,4096]{1,0:T(8,128)(2,1)} async-done(((bf16[128,4096]{1,0:T(8,128)(2,1)}), bf16[512,4096]{1,0:T(8,128)(2,1)}) %all-gather.17.cloned.1.call-update) | async-done | bytes 4194320 | tf_op jit(solution)/shard_map/all_gather | solution.py:44
  92.5 119.6 %all-gather.15.cloned.1.call-done = bf16[4096,2752]{0,1:T(8,128)(2,1)} async-done(((bf16[512,2752]{0,1:T(8,128)(2,1)}), bf16[4096,2752]{0,1:T(8,128)(2,1)}) %all-gather.15.cloned.1.call-update) | async-done | bytes 22544400 | tf_op jit(solution)/shard_map/all_gather | solution.py:26
  212.1 18.6 %fusion.10 = bf16[512,2752]{0,1:T(8,128)(2,1)} fusion(bf16[4096,2752]{0,1:T(8,128)(2,1)} %all-gather.15.cloned.1.call-done, bf16[512,4096]{1,0:T(8,128)(2,1)} %all-gather.17.cloned.1.call-done), kind=kOutput, calls=%fused_computation.22 | convolution fusion | flops 11544133632 | bytes 29556736 | tf_op jit(solution)/shard_map/dot_general | solution.py:50
  230.7 102.3 %all-gather.19.cloned.1.call-done = bf16[4096,2752]{0,1:T(8,128)(2,1)} async-done(((bf16[512,2752]{0,1:T(8,128)(2,1)}), bf16[4096,2752]{0,1:T(8,128)(2,1)}) %all-gather.19.cloned.1.call-update) | async-done | bytes 22544400 | tf_op jit(solution)/shard_map/all_gather | solution.py:26
  333.0 18.6 %fusion.11 = bf16[512,2752]{0,1:T(8,128)(2,1)} fusion(bf16[4096,2752]{0,1:T(8,128)(2,1)} %all-gather.19.cloned.1.call-done, bf16[512,4096]{1,0:T(8,128)(2,1)} %all-gather.17.cloned.1.call-done), kind=kOutput, calls=%fused_computation.23 | convolution fusion | flops 11544133632 | bytes 29556736 | tf_op jit(solution)/shard_map/dot_general | solution.py:49
  351.5 63.0 %all-gather.13.cloned.1.call-done = bf16[512,4096]{1,0:T(8,128)(2,1)} async-done(((bf16[128,4096]{1,0:T(8,128)(2,1)}), bf16[512,4096]{1,0:T(8,128)(2,1)}) %all-gather.13.cloned.1.call-update) | async-done | bytes 4194320 | tf_op jit(solution)/shard_map/all_gather | solution.py:47
  414.6 119.5 %all-gather.11.cloned.1.call-done = bf16[4096,2752]{0,1:T(8,128)(2,1)} async-done(((bf16[512,2752]{0,1:T(8,128)(2,1)}), bf16[4096,2752]{0,1:T(8,128)(2,1)}) %all-gather.11.cloned.1.call-update) | async-done | bytes 22544400 | tf_op jit(solution)/shard_map/all_gather | solution.py:26
  534.1 18.3 %fusion.9 = bf16[512,2752]{0,1:T(8,128)(2,1)S(1)} fusion(bf16[4096,2752]{0,1:T(8,128)(2,1)} %all-gather.11.cloned.1.call-done, bf16[512,4096]{1,0:T(8,128)(2,1)} %all-gather.13.cloned.1.call-done), kind=kOutput, calls=%fused_computation.21 | convolution fusion | flops 11544133632 | bytes 29556736 | tf_op jit(solution)/shard_map/dot_general | solution.py:54
  552.4 6.4 fusion.4
  558.8 19.7 %fusion.12 = f32[512,4096]{1,0:T(8,128)} fusion(bf16[512,2752]{0,1:T(8,128)(2,1)S(1)} %get-tuple-element.5, bf16[4096,2752]{0,1:T(8,128)(2,1)} %all-gather.19.cloned.1.call-done), kind=kOutput, calls=%fused_computation.27 | convolution fusion | flops 11542724608 | bytes 33751040 | tf_op jit(solution)/shard_map/dot_general | solution.py:12
  578.5 20.7 %convolution_add_fusion = f32[512,4096]{1,0:T(8,128)} fusion(f32[512,4096]{1,0:T(8,128)} %fusion.12, bf16[512,2752]{0,1:T(8,128)(2,1)} %get-tuple-element.6, bf16[4096,2752]{0,1:T(8,128)(2,1)} %all-gather.15.cloned.1.call-done), kind=kOutput, calls=%fused_computation.8 | convolution fusion | flops 11544821760 | bytes 42139648 | tf_op jit(solution)/shard_map/dot_general | solution.py:12
  599.2 0.0 all-gather.25.cloned.1.call-start
  599.3 0.7 all-gather.25.cloned.1.call-update
  600.0 0.0 all-gather.21.cloned.1.call-start
  600.0 0.5 all-gather.21.cloned.1.call-update
  600.5 0.3 all-gather.27.cloned.1.call-start
  600.8 0.5 all-gather.27.cloned.1.call-update
  601.3 59.3 %all-gather.23.cloned.1.call-done = bf16[4096,1024]{1,0:T(8,128)(2,1)} async-done(((bf16[512,1024]{1,0:T(8,128)(2,1)}), bf16[4096,1024]{1,0:T(8,128)(2,1)}) %all-gather.23.cloned.1.call-update) | async-done | bytes 8388624 | tf_op jit(solution)/shard_map/all_gather | solution.py:37
  660.5 8.3 copy.13
  668.8 116.3 %all-gather.29.cloned.1.call-done = bf16[4096,1024]{1,0:T(8,128)(2,1)} async-done(((bf16[512,1024]{1,0:T(8,128)(2,1)}), bf16[4096,1024]{1,0:T(8,128)(2,1)}) %all-gather.29.cloned.1.call-update) | async-done | bytes 8388624 | tf_op jit(solution)/shard_map/all_gather | solution.py:37
  785.1 8.3 copy.16
  793.4 137.3 %reduce-scatter.2.cloned.1.call-done = f32[128,4096]{1,0:T(8,128)} async-done(((f32[512,4096]{1,0:T(8,128)}), f32[128,4096]{1,0:T(8,128)}) %reduce-scatter.2.cloned.1.call-update) | async-done | bytes 2097168 | tf_op jit(solution)/shard_map/reduce_scatter | solution.py:65
  930.8 2.7 convert_element_type.50
  933.5 118.6 %all-gather.25.cloned.1.call-done = bf16[4096,2752]{0,1:T(8,128)(2,1)} async-done(((bf16[512,2752]{0,1:T(8,128)(2,1)}), bf16[4096,2752]{0,1:T(8,128)(2,1)}) %all-gather.25.cloned.1.call-update) | async-done | bytes 22544400 | tf_op jit(solution)/shard_map/all_gather | solution.py:30
  1052.1 30.5 %convolution_bitcast_fusion = f32[1024,2752]{0,1:T(8,128)} fusion(bf16[4096,2752]{0,1:T(8,128)(2,1)} %all-gather.25.cloned.1.call-done, bf16[4096,1024]{1,0:T(8,128)(2,1)} %bitcast.45), kind=kOutput, calls=%fused_computation.6 | convolution fusion | flops 23085449216 | bytes 42205184 | tf_op jit(solution)/shard_map/dot_general | solution.py:18
  1082.6 90.2 %all-gather.21.cloned.1.call-done = bf16[4096,2752]{0,1:T(8,128)(2,1)} async-done(((bf16[512,2752]{0,1:T(8,128)(2,1)}), bf16[4096,2752]{0,1:T(8,128)(2,1)}) %all-gather.21.cloned.1.call-update) | async-done | bytes 22544400 | tf_op jit(solution)/shard_map/all_gather | solution.py:30
  1172.8 30.5 %convolution_bitcast_fusion.1 = f32[1024,2752]{0,1:T(8,128)} fusion(bf16[4096,2752]{0,1:T(8,128)(2,1)} %all-gather.21.cloned.1.call-done, bf16[4096,1024]{1,0:T(8,128)(2,1)} %bitcast.46), kind=kOutput, calls=%fused_computation.7 | convolution fusion | flops 23085449216 | bytes 42205184 | tf_op jit(solution)/shard_map/dot_general | solution.py:18
  1203.3 89.7 %all-gather.27.cloned.1.call-done = bf16[4096,2752]{0,1:T(8,128)(2,1)} async-done(((bf16[512,2752]{0,1:T(8,128)(2,1)}), bf16[4096,2752]{0,1:T(8,128)(2,1)}) %all-gather.27.cloned.1.call-update) | async-done | bytes 22544400 | tf_op jit(solution)/shard_map/all_gather | solution.py:30
  1293.1 30.8 %fusion.13 = f32[2752,1024]{1,0:T(8,128)} fusion(bf16[4096,2752]{0,1:T(8,128)(2,1)} %all-gather.27.cloned.1.call-done, bf16[4096,1024]{1,0:T(8,128)(2,1)} %bitcast.44), kind=kOutput, calls=%fused_computation.28 | convolution fusion | flops 23085449216 | bytes 42205184 | tf_op jit(solution)/shard_map/dot_general | solution.py:18
  (14 shorter events, 0.1 us)
Async XLA Ops:
  7.2 85.3 %all-gather.17.cloned.1.call-start = ((), (), s32[]{:S(2)}) async-start(), calls=%async_computation.6 | async-start | bytes 5242880 | tf_op jit(solution)/shard_map/all_gather | solution.py:44
  7.9 204.2 %all-gather.15.cloned.1.call-start = ((), (), s32[]{:S(2)}) async-start(), calls=%async_computation.5 | async-start | bytes 25362432 | tf_op jit(solution)/shard_map/all_gather | solution.py:26
  11.5 321.4 %all-gather.19.cloned.1.call-start = ((), (), s32[]{:S(2)}) async-start(), calls=%async_computation.7 | async-start | bytes 25362432 | tf_op jit(solution)/shard_map/all_gather | solution.py:26
  15.1 4.3 copy-start.1
  15.1 399.4 %all-gather.13.cloned.1.call-start = ((), (), s32[]{:S(2)}) async-start(), calls=%async_computation.4 | async-start | bytes 5242880 | tf_op jit(solution)/shard_map/all_gather | solution.py:47
  15.7 518.3 %all-gather.11.cloned.1.call-start = ((), (), s32[]{:S(2)}) async-start(), calls=%async_computation.3 | async-start | bytes 25362432 | tf_op jit(solution)/shard_map/all_gather | solution.py:26
  19.3 20.7 %copy-start.2 = (bf16[128,4096]{1,0:T(8,128)(2,1)S(1)}, bf16[128,4096]{1,0:T(8,128)(2,1)}, u32[]{:S(2)}) copy-start(bf16[128,4096]{1,0:T(8,128)(2,1)} %param.9) | copy-start | bytes 3145732
  19.3 641.2 %all-gather.23.cloned.1.call-start = ((), (), s32[]{:S(2)}) async-start(), calls=%async_computation.10 | async-start | bytes 9437184 | tf_op jit(solution)/shard_map/all_gather | solution.py:37
  39.9 745.2 %all-gather.29.cloned.1.call-start = ((), (), s32[]{:S(2)}) async-start(), calls=%async_computation.13 | async-start | bytes 9437184 | tf_op jit(solution)/shard_map/all_gather | solution.py:37
  58.8 872.0 %reduce-scatter.2.cloned.1.call-start = ((), (), s32[]{:S(2)}) async-start(), calls=%async_computation.8 | async-start | bytes 10485760 | tf_op jit(solution)/shard_map/reduce_scatter | solution.py:65
  534.1 18.3 %copy-start.3 = (bf16[512,2752]{0,1:T(8,128)(2,1)S(1)}, bf16[512,2752]{0,1:T(8,128)(2,1)}, u32[]{:S(2)}) copy-start(bf16[512,2752]{0,1:T(8,128)(2,1)} %fusion.11) | copy-start | bytes 8454148
  558.8 19.7 %copy-start = (bf16[512,2752]{0,1:T(8,128)(2,1)}, bf16[512,2752]{0,1:T(8,128)(2,1)S(1)}, u32[]{:S(2)}) copy-start(bf16[512,2752]{0,1:T(8,128)(2,1)S(1)} %get-tuple-element.5) | copy-start | bytes 8454148
  599.2 452.9 %all-gather.25.cloned.1.call-start = ((), (), s32[]{:S(2)}) async-start(), calls=%async_computation.11 | async-start | bytes 25362432 | tf_op jit(solution)/shard_map/all_gather | solution.py:30
  600.0 572.8 %all-gather.21.cloned.1.call-start = ((), (), s32[]{:S(2)}) async-start(), calls=%async_computation.9 | async-start | bytes 25362432 | tf_op jit(solution)/shard_map/all_gather | solution.py:30
  600.5 692.5 %all-gather.27.cloned.1.call-start = ((), (), s32[]{:S(2)}) async-start(), calls=%async_computation.12 | async-start | bytes 25362432 | tf_op jit(solution)/shard_map/all_gather | solution.py:30
Sparse Core Ops, SparseCore 0:
  9.5 82.8 all-gather.16
  94.9 117.1 all-gather.14
  214.6 118.3 all-gather.18
  334.4 80.1 all-gather.12
  416.8 117.1 all-gather.10
  536.6 123.8 all-gather.22
  662.6 122.4 all-gather.28
  788.0 142.6 reduce-scatter.1
  933.2 118.8 all-gather.24
  1054.4 118.3 all-gather.20
  1174.7 118.3 all-gather.26
